TPU v7x, 32 devices: a whole 2x2x4 slice. The times are simulated.
32 devices in a mesh: grp: 2 (over x), ep: 16 (over z, y, core), tp: 1.
Axes of the slice: x: 2, y: 2, z: 4, core: 2. Of those that a mesh axis runs over, the one named last changes fastest.
Arguments:
- tokens: bfloat16 [2048, 1024], P(('grp', 'ep')), parts along dimension 0, may hold values from -6 to 6
- norm_gain: float32 [1024], replicated, may hold values from 0.1 to 1.9
- routes: int32 [2048, 6], P(('grp', 'ep')), parts along dimension 0, may hold values from 0 to 15, all different within a row; in each aligned block of 64 rows (0 to 63, 64 to 127, ...) at most 32 rows name the same one
- gate_weights: float32 [2048, 6], P(('grp', 'ep')), parts along dimension 0, may hold values from 0.1 to 1
- w_gate: bfloat16 [16, 1024, 2048], P('ep', None, 'tp'), may hold values from -0.1875 to 0.1875
- w_up: bfloat16 [16, 1024, 2048], P('ep', None, 'tp'), may hold values from -0.1875 to 0.1875
- w_down: bfloat16 [16, 2048, 1024], P('ep', 'tp'), may hold values from -0.125 to 0.125
Outputs:
- mixed: bfloat16 [2048, 1024], P(('grp', 'ep')), parts along dimension 0
There are 2 independent parts, one for each index of `grp`. A program takes and returns all parts, laid end to end along the dimension named above; an argument that names none is the same for every part. Nothing has to cross between parts.
Inputs may be any that keep to these rules, and one draw needn't show every extreme that they name: `routes`: each row names 6 different experts. Within the rows of one index of ep no expert is named more than 32 times, and in every draw some expert is named exactly 32 times in some index's rows.
All inputs are finite; a program needn't handle non-finite values.
Results may differ from a plain program's by a relative error of at most 0.013.
Values may be sent and summed in bfloat16 or wider, within the bound.
No kernel may reach another device: no remote copies, remote signals or barrier semaphores. Data moves between devices by JAX's collectives and lax.ppermute only.
A program may use at most 64 MiB of HBM per device.

v0:
```python
import jax
import jax.numpy as jnp
from jax import lax
from jax.sharding import PartitionSpec as P


def hidden_rows(rows, w_gate, w_up):
    gate = jnp.dot(rows, w_gate[0], preferred_element_type=jnp.float32)
    up = jnp.dot(rows, w_up[0], preferred_element_type=jnp.float32)
    return (jax.nn.silu(gate) * up).astype(jnp.bfloat16)


def weigh_rows(combine, returned):
    upper = combine.astype(jnp.bfloat16)
    lower = (combine - upper.astype(jnp.float32)).astype(jnp.bfloat16)
    first = jnp.dot(upper, returned, preferred_element_type=jnp.float32)
    return first + jnp.dot(lower, returned, preferred_element_type=jnp.float32)


def shards(tokens, norm_gain, routes, gate_weights, w_gate, w_up, w_down):
    values = tokens.astype(jnp.float32)
    scale = lax.rsqrt(jnp.mean(values * values, axis=-1, keepdims=True) + 1e-06)
    normed = (values * scale * norm_gain).astype(jnp.bfloat16)
    width = tokens.shape[1]
    tok_dev = tokens.shape[0]
    topk = routes.shape[1]
    experts = lax.axis_size("ep")
    capacity = min(tok_dev, max(2, 4 * tok_dev * topk // (3 * experts)))
    expert_ids = jnp.arange(experts, dtype=jnp.int32)
    hits = routes[:, :, None] == expert_ids[None, None, :]
    chosen = jnp.any(hits, axis=1).astype(jnp.int32)
    weight_tok = jnp.sum(jnp.where(hits, gate_weights[:, :, None], 0.0), axis=1)
    rank = jnp.cumsum(chosen, axis=0) - chosen
    slot = jnp.where(chosen > 0, rank * experts + expert_ids[None, :], -1)
    slot_ids = jnp.arange(capacity * experts, dtype=jnp.int32)
    placed = slot[:, :, None] == slot_ids[None, None, :]
    place = jnp.any(placed, axis=1).astype(jnp.bfloat16)
    combine = jnp.sum(jnp.where(placed, weight_tok[:, :, None], 0.0), axis=1)
    dispatch = jnp.dot(place.T, normed, preferred_element_type=jnp.float32)
    dispatch = dispatch.astype(jnp.bfloat16).reshape(capacity, experts, width)
    arrived = lax.all_to_all(dispatch, "ep", split_axis=1, concat_axis=1, tiled=True)
    rows = arrived.reshape(-1, width)
    partial_value = jnp.dot(
        hidden_rows(rows, w_gate, w_up), w_down[0], preferred_element_type=jnp.float32
    )
    output = lax.psum(partial_value.astype(jnp.bfloat16), "tp")
    returned = lax.all_to_all(
        output.reshape(arrived.shape), "ep", split_axis=1, concat_axis=1, tiled=True
    )
    mixed = weigh_rows(combine, returned.reshape(-1, width))
    return mixed.astype(jnp.bfloat16)


def solution(mesh):
    in_specs = (
        P(("grp", "ep"), None),
        P(),
        P(("grp", "ep"), None),
        P(("grp", "ep"), None),
        P("ep", None, "tp"),
        P("ep", None, "tp"),
        P("ep", "tp", None),
    )
    out_specs = P(("grp", "ep"), None)
    return jax.shard_map(shards, mesh=mesh, in_specs=in_specs, out_specs=out_specs, check_vma=False)
```

profile of v0, /device:TPU:11, one launch (start us, length us, event | category | flops | bytes accessed | tf_op | source)
XLA Modules:
  0.0 83.4 jit_solution(14729144316334113847)
XLA Ops:
  0.0 0.7 fusion.23
  0.7 0.1 copy.20
  0.8 0.1 reduce_window_sum.11
  0.9 0.5 fusion.8
  1.5 1.3 %fusion.17 = f32[64]{0:T(128)S(1)} fusion(bf16[64,1024]{1,0:T(8,128)(2,1)} %param.7), kind=kLoop, calls=%fused_computation.16 | loop fusion | flops 196544 | bytes 131328 | tf_op jit(solution)/shard_map/reduce_sum | solution.py:22
  2.8 1.4 %convolution_convert_fusion = bf16[512,1024]{1,0:T(8,128)(2,1)S(1)} fusion(pred[64,512]{1,0:T(8,128)(4,1)S(1)} %fusion.8, bf16[64,1024]{1,0:T(8,128)(2,1)} %param.7, f32[1024]{0:T(1024)} %param.8, f32[64]{0:T(128)S(1)} %add_rsqrt_fusion), kind=kOutput, calls=%fused_computation.10 | convolution fusion | flops 67895296 | bytes 1216768 | tf_op jit(solution)/shard_map/dot_general | solution.py:39
  4.2 0.6 copy.22
  4.8 31.7 %all_to_all.10 = bf16[32,16,1024]{2,0,1:T(8,128)(2,1)S(1)} all-to-all(bf16[32,16,1024]{2,0,1:T(8,128)(2,1)S(1)} %copy.22), channel_id=1, replica_groups=mesh['grp'=2,'ep'=16,'tp'=1] {'ep'}, dimensions={1} | all-to-all | bytes 2097152 | tf_op jit(solution)/shard_map/all_to_all | solution.py:41
  36.5 0.6 copy.23
  37.1 0.0 copy-done.2
  37.1 4.3 %fusion.4 = f32[512,2048]{1,0:T(8,128)} fusion(bf16[512,1024]{1,0:T(8,128)(2,1)S(1)} %bitcast.29, bf16[1,1024,2048]{2,1,0:T(8,128)(2,1)S(1)} %copy-done.2), kind=kOutput, calls=%fused_computation.4 | convolution fusion | flops 2147483648 | bytes 9437184 | tf_op jit(solution)/shard_map/dot_general | solution.py:8
  41.4 9.2 %fusion.11 = bf16[512,1024]{1,0:T(8,128)(2,1)S(1)} fusion(bf16[1,2048,1024]{2,1,0:T(8,128)(2,1)} %param.13, f32[512,2048]{1,0:T(8,128)} %fusion.4, bf16[512,1024]{1,0:T(8,128)(2,1)S(1)} %bitcast.30, bf16[1,1024,2048]{2,1,0:T(8,128)(2,1)} %param.12), kind=kOutput, calls=%fused_computation.11 | convolution fusion | flops 4301783040 | bytes 14680064 | tf_op jit(solution)/shard_map/dot_general | solution.py:43
  50.6 0.0 copy-start
  50.6 0.0 copy-start.1
  50.7 1.6 %copy.24 = bf16[32,16,1024]{2,0,1:T(8,128)(2,1)} copy(bf16[32,16,1024]{2,1,0:T(8,128)(2,1)S(1)} %bitcast.31) | data formatting | bytes 2097152 | tf_op jit(solution)/shard_map/reshape | solution.py:48
  52.2 4.4 %all-to-all-start.1 = ((bf16[32,16,1024]{2,0,1:T(8,128)(2,1)}), bf16[32,16,1024]{2,0,1:T(8,128)(2,1)S(1)}, u32[]{:S(2)}, u32[]{:S(2)}) async-start(bf16[32,16,1024]{2,0,1:T(8,128)(2,1)} %copy.24), calls=%async_computation.1 | async-start | bytes 2097152 | tf_op jit(solution)/shard_map/all_to_all | solution.py:47
  56.6 0.0 copy-done
  56.6 0.0 copy-done.1
  56.7 0.1 copy.21
  56.7 0.6 select_reduce_fusion
  57.4 24.2 %all-to-all-done.1 = bf16[32,16,1024]{2,0,1:T(8,128)(2,1)S(1)} async-done(((bf16[32,16,1024]{2,0,1:T(8,128)(2,1)}), bf16[32,16,1024]{2,0,1:T(8,128)(2,1)S(1)}, u32[]{:S(2)}, u32[]{:S(2)}) %all-to-all-start.1) | async-done | bytes 1048608 | tf_op jit(solution)/shard_map/all_to_all | solution.py:47
  81.5 0.6 copy.25
  82.1 0.3 fusion.25
  82.4 1.0 %fusion.16 = bf16[64,1024]{1,0:T(8,128)(2,1)} fusion(f32[64,1024]{1,0:T(8,128)S(1)} %fusion.25, bf16[512,1024]{1,0:T(8,128)(2,1)S(1)} %bitcast.27, f32[64,512]{1,0:T(8,128)S(1)} %select_reduce_fusion), kind=kOutput, calls=%fused_computation.13 | convolution fusion | flops 67371008 | bytes 1572864 | tf_op jit(solution)/shard_map/dot_general | solution.py:17
  (5 shorter events, 0.0 us)
Async XLA Ops:
  0.9 36.2 %copy-start.2 = (bf16[1,1024,2048]{2,1,0:T(8,128)(2,1)S(1)}, bf16[1,1024,2048]{2,1,0:T(8,128)(2,1)}, u32[]{:S(2)}) copy-start(bf16[1,1024,2048]{2,1,0:T(8,128)(2,1)} %param.11) | copy-start | bytes 12582916
  50.6 6.0 %copy-start = (s32[64,6]{0,1:T(8,128)S(1)}, s32[64,6]{0,1:T(8,128)}, u32[]{:S(2)}) copy-start(s32[64,6]{0,1:T(8,128)} %param.9) | copy-start | bytes 4612
  50.6 6.0 %copy-start.1 = (f32[64,6]{0,1:T(8,128)S(1)}, f32[64,6]{0,1:T(8,128)}, u32[]{:S(2)}) copy-start(f32[64,6]{0,1:T(8,128)} %param.10) | copy-start | bytes 4612
  52.2 29.3 %all-to-all-start.1 = ((bf16[32,16,1024]{2,0,1:T(8,128)(2,1)}), bf16[32,16,1024]{2,0,1:T(8,128)(2,1)S(1)}, u32[]{:S(2)}, u32[]{:S(2)}) async-start(bf16[32,16,1024]{2,0,1:T(8,128)(2,1)} %copy.24), calls=%async_computation.1 | async-start | bytes 2097152 | tf_op jit(solution)/shard_map/all_to_all | solution.py:47
where the time goes:
time: 83.7 us; the launch traced here: 83.4 us
  blocking collectives  31.7 us (38%)
  waiting for transfers between devices  24.2 us (29%)
  matrix products  16.2 us (19%)
  starting transfers between devices  4.39 us (5%)
  local copies, waits for them, and re-layouts  3.51 us (4%)
  other arithmetic  3.31 us (4%)
    all_to_all x1, blocking collectives, shards(): lax.all_to_all(dispatch, 'ep', split_axis=1, concat_axis=1, tiled=True)  31.7 us
    all_to_all x1, waiting for transfers between devices, shards(): lax.all_to_all(output.reshape(arrived.shape), 'ep', split_axis=1, concat_...  24.2 us
    dot_general x1, matrix products, shards(): jnp.dot(hidden_rows(rows, w_gate, w_up), w_down[0], preferred_element_typ...  9.21 us
    all_to_all x1, starting transfers between devices, shards(): lax.all_to_all(output.reshape(arrived.shape), 'ep', split_axis=1, concat_...  4.39 us
    dot_general x1, matrix products, hidden_rows(): gate = jnp.dot(rows, w_gate[0], preferred_element_type=jnp.float32)  4.29 us
  transfers between devices with their start and end apart: 1, of which 1 were waited for; matrix products, arithmetic and copies ran while one was open for 1% of the time, Pallas kernels for 0%

commit v1 on v0

--- a/solution.py
+++ b/solution.py
@@ -44,9 +44,20 @@
         hidden_rows(rows, w_gate, w_up), w_down[0], preferred_element_type=jnp.float32
     )
     output = lax.psum(partial_value.astype(jnp.bfloat16), "tp")
-    returned = lax.all_to_all(
-        output.reshape(arrived.shape), "ep", split_axis=1, concat_axis=1, tiled=True
-    )
+    shard = output.reshape(arrived.shape)
+    ways, here = (lax.axis_size("ep"), lax.axis_index("ep"))
+    width_2 = shard.shape[1] // ways
+    dims = list(shard.shape)
+    dims[1] = width_2
+    height = dims[1]
+    dims[1] = height * ways
+    full = jnp.zeros(dims, shard.dtype)
+    for mask in range(ways):
+        part = lax.dynamic_slice_in_dim(shard, (here ^ mask) * width_2, width_2, axis=1)
+        if mask:
+            part = lax.ppermute(part, "ep", [(d, d ^ mask) for d in range(ways)])
+        full = lax.dynamic_update_slice_in_dim(full, part, (here ^ mask) * height, axis=1)
+    returned = full
     mixed = weigh_rows(combine, returned.reshape(-1, width))
     return mixed.astype(jnp.bfloat16)
 

time: 83.7 us -> 122 us (1.46)
  the two profiles are of different devices: /device:TPU:11 before, /device:TPU:7 now
where the time goes in v1:
time: 122 us; the launch traced here: 121 us
  waiting for transfers between devices  41 us (34%)
  starting transfers between devices  32.5 us (27%)
  local copies, waits for them, and re-layouts  26.3 us (22%)
  matrix products  18.4 us (15%)
  other arithmetic  3.04 us (2%)
    ppermute x15, starting transfers between devices, shards(): part = lax.ppermute(part, 'ep', [(d, d ^ mask) for d in range(ways)])  25.9 us
    all_to_all x1, waiting for transfers between devices, shards(): lax.all_to_all(dispatch, 'ep', split_axis=1, concat_axis=1, tiled=True)  23.5 us
    dynamic_update_slice x16, local copies, waits for them, and re-layouts, shards(): lax.dynamic_update_slice_in_dim(full, part, (here ^ mask) * height, axis=1)  21 us
    ppermute x15, waiting for transfers between devices, shards(): part = lax.ppermute(part, 'ep', [(d, d ^ mask) for d in range(ways)])  17.4 us
    dot_general x1, matrix products, shards(): jnp.dot(hidden_rows(rows, w_gate, w_up), w_down[0], preferred_element_typ...  9.22 us
    all_to_all x1, starting transfers between devices, shards(): lax.all_to_all(dispatch, 'ep', split_axis=1, concat_axis=1, tiled=True)  6.63 us
    dot_general x1, matrix products, hidden_rows(): gate = jnp.dot(rows, w_gate[0], preferred_element_type=jnp.float32)  6.46 us
    dynamic_slice x1, local copies, waits for them, and re-layouts, shards(): lax.dynamic_slice_in_dim(shard, (here ^ mask) * width_2, width_2, axis=1)  2.78 us
  transfers between devices with their start and end apart: 16, of which 6 were waited for; matrix products, arithmetic and copies ran while one was open for 17% of the time, Pallas kernels for 0%

profile of v1, /device:TPU:7, one launch (start us, length us, event | category | flops | bytes accessed | tf_op | source)
XLA Modules:
  0.0 121.4 jit_solution(3952338239339115520)
XLA Ops:
  2.5 1.4 %convolution_convert_fusion = bf16[512,1024]{1,0:T(8,128)(2,1)S(1)} fusion(pred[64,512]{1,0:T(8,128)(4,1)S(1)} %fusion.8, bf16[64,1024]{1,0:T(8,128)(2,1)} %param.7, f32[1024]{0:T(1024)} %param.8, f32[64]{0:T(128)S(1)} %add_rsqrt_fusion), kind=kOutput, calls=%fused_computation.10 | convolution fusion | flops 67895296 | bytes 1216768 | tf_op jit(solution)/shard_map/dot_general | solution.py:39
  3.9 1.6 %copy.19 = bf16[32,16,1024]{2,0,1:T(8,128)(2,1)} copy(bf16[32,16,1024]{2,1,0:T(8,128)(2,1)S(1)} %bitcast.29) | data formatting | bytes 2097152 | tf_op jit(solution)/shard_map/reshape | solution.py:40
  5.5 6.6 %all-to-all-start = ((bf16[32,16,1024]{2,0,1:T(8,128)(2,1)}), bf16[32,16,1024]{2,0,1:T(8,128)(2,1)S(1)}, u32[]{:S(2)}, u32[]{:S(2)}) async-start(bf16[32,16,1024]{2,0,1:T(8,128)(2,1)} %copy.19), calls=%async_computation | async-start | bytes 2097152 | tf_op jit(solution)/shard_map/all_to_all | solution.py:41
  12.1 23.5 %all-to-all-done = bf16[32,16,1024]{2,0,1:T(8,128)(2,1)S(1)} async-done(((bf16[32,16,1024]{2,0,1:T(8,128)(2,1)}), bf16[32,16,1024]{2,0,1:T(8,128)(2,1)S(1)}, u32[]{:S(2)}, u32[]{:S(2)}) %all-to-all-start) | async-done | bytes 1048608 | tf_op jit(solution)/shard_map/all_to_all | solution.py:41
  36.2 6.5 %fusion.4 = f32[512,2048]{1,0:T(8,128)} fusion(bf16[512,1024]{1,0:T(8,128)(2,1)S(1)} %bitcast.30, bf16[1,1024,2048]{2,1,0:T(8,128)(2,1)} %param.11), kind=kOutput, calls=%fused_computation.4 | convolution fusion | flops 2147483648 | bytes 9437184 | tf_op jit(solution)/shard_map/dot_general | solution.py:8
  42.7 9.2 %fusion.11 = bf16[512,1024]{1,0:T(8,128)(2,1)S(1)} fusion(bf16[1,2048,1024]{2,1,0:T(8,128)(2,1)} %param.13, f32[512,2048]{1,0:T(8,128)} %fusion.4, bf16[512,1024]{1,0:T(8,128)(2,1)S(1)} %bitcast.31, bf16[1,1024,2048]{2,1,0:T(8,128)(2,1)} %param.12), kind=kOutput, calls=%fused_computation.11 | convolution fusion | flops 4301783040 | bytes 14680064 | tf_op jit(solution)/shard_map/dot_general | solution.py:43
  51.9 2.8 %constant_dynamic-slice_fusion = (bf16[32,1,1024]{2,1,0:T(2,128)(2,1)S(1)}, bf16[32,1,1024]{2,1,0:T(2,128)(2,1)S(1)}, bf16[32,1,1024]{2,1,0:T(2,128)(2,1)S(1)}, ...) fusion(bf16[32,16,1024]{2,1,0:T(8,128)(2,1)S(1)} %bitcast.28, ...), kind=kLoop, calls=%fused_computation.29 | loop fusion | bytes 2097216 | tf_op jit(solution)/shard_map/dynamic_slice | solution.py:56
  54.9 2.0 %collective-permute-start.2 = (bf16[32,1,1024]{2,1,0:T(2,128)(2,1)S(1)}, bf16[32,1,1024]{2,1,0:T(2,128)(2,1)S(1)}, u32[]{:S(2)}, u32[]{:S(2)}) collective-permute-start(bf16[32,1,1024]{2,1,0:T(2,128)(2,1)S(1)} %get-tuple-element.17), channel_id=1, source_target_pairs={{0,3},{1,2},{2,1},{3,0},{4,7},{5,6},{6,5},{7,4},{8,11},{9,10},{10,... | collective-permute-start | bytes 196616 | tf_op jit(solution)/shard_map/ppermute | solution.py:58
  56.9 2.5 %collective-permute-start.3 = (bf16[32,1,1024]{2,1,0:T(2,128)(2,1)S(1)}, bf16[32,1,1024]{2,1,0:T(2,128)(2,1)S(1)}, u32[]{:S(2)}, u32[]{:S(2)}) collective-permute-start(bf16[32,1,1024]{2,1,0:T(2,128)(2,1)S(1)} %get-tuple-element.16), channel_id=1, source_target_pairs={{0,4},{1,5},{2,6},{3,7},{4,0},{5,1},{6,2},{7,3},{8,12},{9,13},{10,... | collective-permute-start | bytes 196616 | tf_op jit(solution)/shard_map/ppermute | solution.py:58
  59.4 1.5 %collective-permute-start.5 = (bf16[32,1,1024]{2,1,0:T(2,128)(2,1)S(1)}, bf16[32,1,1024]{2,1,0:T(2,128)(2,1)S(1)}, u32[]{:S(2)}, u32[]{:S(2)}) collective-permute-start(bf16[32,1,1024]{2,1,0:T(2,128)(2,1)S(1)} %get-tuple-element.14), channel_id=1, source_target_pairs={{0,6},{1,7},{2,4},{3,5},{4,2},{5,3},{6,0},{7,1},{8,14},{9,15},{10,... | collective-permute-start | bytes 196616 | tf_op jit(solution)/shard_map/ppermute | solution.py:58
  61.0 3.2 %collective-permute-start.6 = (bf16[32,1,1024]{2,1,0:T(2,128)(2,1)S(1)}, bf16[32,1,1024]{2,1,0:T(2,128)(2,1)S(1)}, u32[]{:S(2)}, u32[]{:S(2)}) collective-permute-start(bf16[32,1,1024]{2,1,0:T(2,128)(2,1)S(1)} %get-tuple-element.13), channel_id=1, source_target_pairs={{0,7},{1,6},{2,5},{3,4},{4,3},{5,2},{6,1},{7,0},{8,15},{9,14},{10,... | collective-permute-start | bytes 196616 | tf_op jit(solution)/shard_map/ppermute | solution.py:58
  64.1 1.9 %collective-permute-start.7 = (bf16[32,1,1024]{2,1,0:T(2,128)(2,1)S(1)}, bf16[32,1,1024]{2,1,0:T(2,128)(2,1)S(1)}, u32[]{:S(2)}, u32[]{:S(2)}) collective-permute-start(bf16[32,1,1024]{2,1,0:T(2,128)(2,1)S(1)} %get-tuple-element.12), channel_id=1, source_target_pairs={{0,8},{1,9},{2,10},{3,11},{4,12},{5,13},{6,14},{7,15},{8,0},{9,1},... | collective-permute-start | bytes 196616 | tf_op jit(solution)/shard_map/ppermute | solution.py:58
  66.3 3.3 %collective-permute-start.9 = (bf16[32,1,1024]{2,1,0:T(2,128)(2,1)S(1)}, bf16[32,1,1024]{2,1,0:T(2,128)(2,1)S(1)}, u32[]{:S(2)}, u32[]{:S(2)}) collective-permute-start(bf16[32,1,1024]{2,1,0:T(2,128)(2,1)S(1)} %get-tuple-element.10), channel_id=1, source_target_pairs={{0,10},{1,11},{2,8},{3,9},{4,14},{5,15},{6,12},{7,13},{8,2},{9,3},... | collective-permute-start | bytes 196616 | tf_op jit(solution)/shard_map/ppermute | solution.py:58
  69.7 5.3 %collective-permute-done.5 = bf16[32,1,1024]{2,1,0:T(2,128)(2,1)S(1)} collective-permute-done((bf16[32,1,1024]{2,1,0:T(2,128)(2,1)S(1)}, bf16[32,1,1024]{2,1,0:T(2,128)(2,1)S(1)}, u32[]{:S(2)}, u32[]{:S(2)}) %collective-permute-start.5) | collective-permute-done | bytes 65568 | tf_op jit(solution)/shard_map/ppermute | solution.py:58
  75.5 2.3 %collective-permute-done.6 = bf16[32,1,1024]{2,1,0:T(2,128)(2,1)S(1)} collective-permute-done((bf16[32,1,1024]{2,1,0:T(2,128)(2,1)S(1)}, bf16[32,1,1024]{2,1,0:T(2,128)(2,1)S(1)}, u32[]{:S(2)}, u32[]{:S(2)}) %collective-permute-start.6) | collective-permute-done | bytes 65568 | tf_op jit(solution)/shard_map/ppermute | solution.py:58
  77.8 1.8 %collective-permute-start.11 = (bf16[32,1,1024]{2,1,0:T(2,128)(2,1)S(1)}, bf16[32,1,1024]{2,1,0:T(2,128)(2,1)}, u32[]{:S(2)}, u32[]{:S(2)}) collective-permute-start(bf16[32,1,1024]{2,1,0:T(2,128)(2,1)S(1)} %get-tuple-element.8), channel_id=1, source_target_pairs={{0,12},{1,13},{2,14},{3,15},{4,8},{5,9},{6,10},{7,11},{8,4},{9,5},... | collective-permute-start | bytes 196616 | tf_op jit(solution)/shard_map/ppermute | solution.py:58
  79.6 2.0 %collective-permute-start.12 = (bf16[32,1,1024]{2,1,0:T(2,128)(2,1)S(1)}, bf16[32,1,1024]{2,1,0:T(2,128)(2,1)}, u32[]{:S(2)}, u32[]{:S(2)}) collective-permute-start(bf16[32,1,1024]{2,1,0:T(2,128)(2,1)S(1)} %get-tuple-element.7), channel_id=1, source_target_pairs={{0,13},{1,12},{2,15},{3,14},{4,9},{5,8},{6,11},{7,10},{8,5},{9,4},... | collective-permute-start | bytes 196616 | tf_op jit(solution)/shard_map/ppermute | solution.py:58
  81.6 8.3 %collective-permute-done.8 = bf16[32,1,1024]{2,1,0:T(2,128)(2,1)S(1)} collective-permute-done((bf16[32,1,1024]{2,1,0:T(2,128)(2,1)S(1)}, bf16[32,1,1024]{2,1,0:T(2,128)(2,1)S(1)}, u32[]{:S(2)}, u32[]{:S(2)}) %collective-permute-start.8) | collective-permute-done | bytes 65568 | tf_op jit(solution)/shard_map/ppermute | solution.py:58
  89.9 2.5 %collective-permute-start.13 = (bf16[32,1,1024]{2,1,0:T(2,128)(2,1)S(1)}, bf16[32,1,1024]{2,1,0:T(2,128)(2,1)}, u32[]{:S(2)}, u32[]{:S(2)}) collective-permute-start(bf16[32,1,1024]{2,1,0:T(2,128)(2,1)S(1)} %get-tuple-element.6), channel_id=1, source_target_pairs={{0,14},{1,15},{2,12},{3,13},{4,10},{5,11},{6,8},{7,9},{8,6},{9,7},... | collective-permute-start | bytes 196616 | tf_op jit(solution)/shard_map/ppermute | solution.py:58
  93.8 4.4 %collective-permute-start.14 = (bf16[32,1,1024]{2,1,0:T(2,128)(2,1)S(1)}, bf16[32,1,1024]{2,1,0:T(2,128)(2,1)S(1)}, u32[]{:S(2)}, u32[]{:S(2)}) collective-permute-start(bf16[32,1,1024]{2,1,0:T(2,128)(2,1)S(1)} %get-tuple-element.5), channel_id=1, source_target_pairs={{0,15},{1,14},{2,13},{3,12},{4,11},{5,10},{6,9},{7,8},{8,7},{9,6},... | collective-permute-start | bytes 196616 | tf_op jit(solution)/shard_map/ppermute | solution.py:58
  110.1 2.2 %dynamic_update_slice.59 = bf16[32,16,1024]{2,1,0:T(8,128)(2,1)S(1)} dynamic-update-slice(bf16[32,16,1024]{2,1,0:T(8,128)(2,1)S(1)} %dynamic_update_slice.58, bf16[32,1,1024]{2,1,0:T(2,128)(2,1)} %collective-permute-done.10, s32[]{:T(128)} %constant.26.clone.1, s32[]{:T(128)S(6)} %select_n.94, s32[]{:T(128)} %constant.26.clone.1) | dynamic-update-slice | bytes 131076 | tf_op jit(solution)/shard_map/dynamic_update_slice | solution.py:59
  112.3 2.2 %dynamic_update_slice.60 = bf16[32,16,1024]{2,1,0:T(8,128)(2,1)S(1)} dynamic-update-slice(bf16[32,16,1024]{2,1,0:T(8,128)(2,1)S(1)} %dynamic_update_slice.59, bf16[32,1,1024]{2,1,0:T(2,128)(2,1)} %collective-permute-done.11, s32[]{:T(128)} %constant.26.clone.1, s32[]{:T(128)S(6)} %select_n.95, s32[]{:T(128)} %constant.26.clone.1) | dynamic-update-slice | bytes 131076 | tf_op jit(solution)/shard_map/dynamic_update_slice | solution.py:59
  114.6 2.2 %dynamic_update_slice.61 = bf16[32,16,1024]{2,1,0:T(8,128)(2,1)S(1)} dynamic-update-slice(bf16[32,16,1024]{2,1,0:T(8,128)(2,1)S(1)} %dynamic_update_slice.60, bf16[32,1,1024]{2,1,0:T(2,128)(2,1)} %collective-permute-done.12, s32[]{:T(128)} %constant.26.clone.1, s32[]{:T(128)S(6)} %select_n.96, s32[]{:T(128)} %constant.26.clone.1) | dynamic-update-slice | bytes 131076 | tf_op jit(solution)/shard_map/dynamic_update_slice | solution.py:59
  116.9 2.2 %dynamic_update_slice.62 = bf16[32,16,1024]{2,1,0:T(8,128)(2,1)S(1)} dynamic-update-slice(bf16[32,16,1024]{2,1,0:T(8,128)(2,1)S(1)} %dynamic_update_slice.61, bf16[32,1,1024]{2,1,0:T(2,128)(2,1)} %collective-permute-done.13, s32[]{:T(128)} %constant.26.clone.1, s32[]{:T(128)S(6)} %select_n.97, s32[]{:T(128)} %constant.26.clone.1) | dynamic-update-slice | bytes 131076 | tf_op jit(solution)/shard_map/dynamic_update_slice | solution.py:59
  (48 shorter events, 19.4 us)
Async XLA Ops:
  5.5 30.2 %all-to-all-start = ((bf16[32,16,1024]{2,0,1:T(8,128)(2,1)}), bf16[32,16,1024]{2,0,1:T(8,128)(2,1)S(1)}, u32[]{:S(2)}, u32[]{:S(2)}) async-start(bf16[32,16,1024]{2,0,1:T(8,128)(2,1)} %copy.19), calls=%async_computation | async-start | bytes 2097152 | tf_op jit(solution)/shard_map/all_to_all | solution.py:41
  51.9 17.7 %copy-start = (s32[64,6]{0,1:T(8,128)S(1)}, s32[64,6]{0,1:T(8,128)}, u32[]{:S(2)}) copy-start(s32[64,6]{0,1:T(8,128)} %param.9) | copy-start | bytes 4612
  51.9 17.7 %copy-start.1 = (f32[64,6]{0,1:T(8,128)S(1)}, f32[64,6]{0,1:T(8,128)}, u32[]{:S(2)}) copy-start(f32[64,6]{0,1:T(8,128)} %param.10) | copy-start | bytes 4612
  54.7 4.7 %collective-permute-start = (bf16[32,1,1024]{2,1,0:T(2,128)(2,1)S(1)}, bf16[32,1,1024]{2,1,0:T(2,128)(2,1)S(1)}, u32[]{:S(2)}, u32[]{:S(2)}) collective-permute-start(bf16[32,1,1024]{2,1,0:T(2,128)(2,1)S(1)} %get-tuple-element.19), channel_id=1, source_target_pairs={{0,1},{1,0},{2,3},{3,2},{4,5},{5,4},{6,7},{7,6},{8,9},{9,8},{10,11... | collective-permute-start | bytes 196616 | tf_op jit(solution)/shard_map/ppermute | solution.py:58
  54.8 6.2 %collective-permute-start.1 = (bf16[32,1,1024]{2,1,0:T(2,128)(2,1)S(1)}, bf16[32,1,1024]{2,1,0:T(2,128)(2,1)S(1)}, u32[]{:S(2)}, u32[]{:S(2)}) collective-permute-start(bf16[32,1,1024]{2,1,0:T(2,128)(2,1)S(1)} %get-tuple-element.18), channel_id=1, source_target_pairs={{0,2},{1,3},{2,0},{3,1},{4,6},{5,7},{6,4},{7,5},{8,10},{9,11},{10,... | collective-permute-start | bytes 196616 | tf_op jit(solution)/shard_map/ppermute | solution.py:58
  54.9 9.3 %collective-permute-start.2 = (bf16[32,1,1024]{2,1,0:T(2,128)(2,1)S(1)}, bf16[32,1,1024]{2,1,0:T(2,128)(2,1)S(1)}, u32[]{:S(2)}, u32[]{:S(2)}) collective-permute-start(bf16[32,1,1024]{2,1,0:T(2,128)(2,1)S(1)} %get-tuple-element.17), channel_id=1, source_target_pairs={{0,3},{1,2},{2,1},{3,0},{4,7},{5,6},{6,5},{7,4},{8,11},{9,10},{10,... | collective-permute-start | bytes 196616 | tf_op jit(solution)/shard_map/ppermute | solution.py:58
  56.9 9.1 %collective-permute-start.3 = (bf16[32,1,1024]{2,1,0:T(2,128)(2,1)S(1)}, bf16[32,1,1024]{2,1,0:T(2,128)(2,1)S(1)}, u32[]{:S(2)}, u32[]{:S(2)}) collective-permute-start(bf16[32,1,1024]{2,1,0:T(2,128)(2,1)S(1)} %get-tuple-element.16), channel_id=1, source_target_pairs={{0,4},{1,5},{2,6},{3,7},{4,0},{5,1},{6,2},{7,3},{8,12},{9,13},{10,... | collective-permute-start | bytes 196616 | tf_op jit(solution)/shard_map/ppermute | solution.py:58
  59.4 6.8 %collective-permute-start.4 = (bf16[32,1,1024]{2,1,0:T(2,128)(2,1)S(1)}, bf16[32,1,1024]{2,1,0:T(2,128)(2,1)S(1)}, u32[]{:S(2)}, u32[]{:S(2)}) collective-permute-start(bf16[32,1,1024]{2,1,0:T(2,128)(2,1)S(1)} %get-tuple-element.15), channel_id=1, source_target_pairs={{0,5},{1,4},{2,7},{3,6},{4,1},{5,0},{6,3},{7,2},{8,13},{9,12},{10,... | collective-permute-start | bytes 196616 | tf_op jit(solution)/shard_map/ppermute | solution.py:58
  59.4 15.6 %collective-permute-start.5 = (bf16[32,1,1024]{2,1,0:T(2,128)(2,1)S(1)}, bf16[32,1,1024]{2,1,0:T(2,128)(2,1)S(1)}, u32[]{:S(2)}, u32[]{:S(2)}) collective-permute-start(bf16[32,1,1024]{2,1,0:T(2,128)(2,1)S(1)} %get-tuple-element.14), channel_id=1, source_target_pairs={{0,6},{1,7},{2,4},{3,5},{4,2},{5,3},{6,0},{7,1},{8,14},{9,15},{10,... | collective-permute-start | bytes 196616 | tf_op jit(solution)/shard_map/ppermute | solution.py:58
  61.0 16.8 %collective-permute-start.6 = (bf16[32,1,1024]{2,1,0:T(2,128)(2,1)S(1)}, bf16[32,1,1024]{2,1,0:T(2,128)(2,1)S(1)}, u32[]{:S(2)}, u32[]{:S(2)}) collective-permute-start(bf16[32,1,1024]{2,1,0:T(2,128)(2,1)S(1)} %get-tuple-element.13), channel_id=1, source_target_pairs={{0,7},{1,6},{2,5},{3,4},{4,3},{5,2},{6,1},{7,0},{8,15},{9,14},{10,... | collective-permute-start | bytes 196616 | tf_op jit(solution)/shard_map/ppermute | solution.py:58
  64.1 15.5 %collective-permute-start.7 = (bf16[32,1,1024]{2,1,0:T(2,128)(2,1)S(1)}, bf16[32,1,1024]{2,1,0:T(2,128)(2,1)S(1)}, u32[]{:S(2)}, u32[]{:S(2)}) collective-permute-start(bf16[32,1,1024]{2,1,0:T(2,128)(2,1)S(1)} %get-tuple-element.12), channel_id=1, source_target_pairs={{0,8},{1,9},{2,10},{3,11},{4,12},{5,13},{6,14},{7,15},{8,0},{9,1},... | collective-permute-start | bytes 196616 | tf_op jit(solution)/shard_map/ppermute | solution.py:58
  66.0 23.9 %collective-permute-start.8 = (bf16[32,1,1024]{2,1,0:T(2,128)(2,1)S(1)}, bf16[32,1,1024]{2,1,0:T(2,128)(2,1)S(1)}, u32[]{:S(2)}, u32[]{:S(2)}) collective-permute-start(bf16[32,1,1024]{2,1,0:T(2,128)(2,1)S(1)} %get-tuple-element.11), channel_id=1, source_target_pairs={{0,9},{1,8},{2,11},{3,10},{4,13},{5,12},{6,15},{7,14},{8,1},{9,0},... | collective-permute-start | bytes 196616 | tf_op jit(solution)/shard_map/ppermute | solution.py:58
  66.3 27.5 %collective-permute-start.9 = (bf16[32,1,1024]{2,1,0:T(2,128)(2,1)S(1)}, bf16[32,1,1024]{2,1,0:T(2,128)(2,1)S(1)}, u32[]{:S(2)}, u32[]{:S(2)}) collective-permute-start(bf16[32,1,1024]{2,1,0:T(2,128)(2,1)S(1)} %get-tuple-element.10), channel_id=1, source_target_pairs={{0,10},{1,11},{2,8},{3,9},{4,14},{5,15},{6,12},{7,13},{8,2},{9,3},... | collective-permute-start | bytes 196616 | tf_op jit(solution)/shard_map/ppermute | solution.py:58
  75.0 35.1 %collective-permute-start.10 = (bf16[32,1,1024]{2,1,0:T(2,128)(2,1)S(1)}, bf16[32,1,1024]{2,1,0:T(2,128)(2,1)}, u32[]{:S(2)}, u32[]{:S(2)}) collective-permute-start(bf16[32,1,1024]{2,1,0:T(2,128)(2,1)S(1)} %get-tuple-element.9), channel_id=1, source_target_pairs={{0,11},{1,10},{2,9},{3,8},{4,15},{5,14},{6,13},{7,12},{8,3},{9,2},... | collective-permute-start | bytes 196616 | tf_op jit(solution)/shard_map/ppermute | solution.py:58
  77.8 34.6 %collective-permute-start.11 = (bf16[32,1,1024]{2,1,0:T(2,128)(2,1)S(1)}, bf16[32,1,1024]{2,1,0:T(2,128)(2,1)}, u32[]{:S(2)}, u32[]{:S(2)}) collective-permute-start(bf16[32,1,1024]{2,1,0:T(2,128)(2,1)S(1)} %get-tuple-element.8), channel_id=1, source_target_pairs={{0,12},{1,13},{2,14},{3,15},{4,8},{5,9},{6,10},{7,11},{8,4},{9,5},... | collective-permute-start | bytes 196616 | tf_op jit(solution)/shard_map/ppermute | solution.py:58
  79.6 35.0 %collective-permute-start.12 = (bf16[32,1,1024]{2,1,0:T(2,128)(2,1)S(1)}, bf16[32,1,1024]{2,1,0:T(2,128)(2,1)}, u32[]{:S(2)}, u32[]{:S(2)}) collective-permute-start(bf16[32,1,1024]{2,1,0:T(2,128)(2,1)S(1)} %get-tuple-element.7), channel_id=1, source_target_pairs={{0,13},{1,12},{2,15},{3,14},{4,9},{5,8},{6,11},{7,10},{8,5},{9,4},... | collective-permute-start | bytes 196616 | tf_op jit(solution)/shard_map/ppermute | solution.py:58
  89.9 26.9 %collective-permute-start.13 = (bf16[32,1,1024]{2,1,0:T(2,128)(2,1)S(1)}, bf16[32,1,1024]{2,1,0:T(2,128)(2,1)}, u32[]{:S(2)}, u32[]{:S(2)}) collective-permute-start(bf16[32,1,1024]{2,1,0:T(2,128)(2,1)S(1)} %get-tuple-element.6), channel_id=1, source_target_pairs={{0,14},{1,15},{2,12},{3,13},{4,10},{5,11},{6,8},{7,9},{8,6},{9,7},... | collective-permute-start | bytes 196616 | tf_op jit(solution)/shard_map/ppermute | solution.py:58
  93.8 25.4 %collective-permute-start.14 = (bf16[32,1,1024]{2,1,0:T(2,128)(2,1)S(1)}, bf16[32,1,1024]{2,1,0:T(2,128)(2,1)S(1)}, u32[]{:S(2)}, u32[]{:S(2)}) collective-permute-start(bf16[32,1,1024]{2,1,0:T(2,128)(2,1)S(1)} %get-tuple-element.5), channel_id=1, source_target_pairs={{0,15},{1,14},{2,13},{3,12},{4,11},{5,10},{6,9},{7,8},{8,7},{9,6},... | collective-permute-start | bytes 196616 | tf_op jit(solution)/shard_map/ppermute | solution.py:58
